TPU v7x, 32 devices: a whole 2x2x4 slice. The times are simulated.
32 devices in a mesh: ep: 4 (over y, x), tp: 8 (over z, core).
Axes of the slice: x: 2, y: 2, z: 4, core: 2. Of those that a mesh axis runs over, the one named last changes fastest.
Arguments:
- queries: bfloat16 [4096, 1024], P('ep', 'tp'), may hold values from -6 to 6
- keys: bfloat16 [4096, 256], P('ep'), may hold values from -6 to 6, as said below
- values: bfloat16 [4096, 256], P('ep'), may hold values from -6 to 6
- slopes: float32 [16], P('tp'), may hold values from 0.002 to 0.08
- sinks: float32 [16], P('tp'), may hold values from 2 to 6
- out_weight: bfloat16 [1024, 2048], P('tp'), may hold values from -0.1875 to 0.1875
- mix_gain: float32 [2048], replicated, may hold values from 0.1 to 1.9
- moe_input: bfloat16 [4096, 2048], P(('ep', 'tp')), may hold values from -6 to 6
- in_gain: float32 [2048], replicated, may hold values from 0.1 to 1.9
- out_gain: float32 [2048], replicated, may hold values from 0.1 to 1.9
- group_router: bfloat16 [2048, 4], replicated, may hold values from -0.125 to 0.125
- expert_router: bfloat16 [2048, 4], replicated, may hold values from -0.125 to 0.125
- routes: int32 [4096, 2], P(('ep', 'tp')), may hold values from 0 to 3, all different within a row; in each aligned block of 128 rows (0 to 127, 128 to 255, ...) at most 96 rows name the same one
- gate_weight: bfloat16 [4, 2048, 1024], P('ep', None, 'tp'), may hold values from -0.125 to 0.125
- up_weight: bfloat16 [4, 2048, 1024], P('ep', None, 'tp'), may hold values from -0.125 to 0.125
- down_weight: bfloat16 [4, 2048, 1024], P('ep', None, 'tp'), may hold values from -0.1875 to 0.1875
Outputs:
- mixer_output: bfloat16 [4096, 2048], P(('ep', 'tp'))
- moe_output: bfloat16 [4096, 2048], P(('ep', 'tp'))
Inputs may be any that keep to these rules, and one draw needn't show every extreme that they name: `keys`: keys share one value range with the queries. `routes`: A token names 2 different experts. Among the rows of one device no expert is named more than 96 times, a bound that some block reaches in every draw.
All inputs are finite; a program needn't handle non-finite values.
Results may differ from a plain program's by a relative error of at most 0.018.
Values may be sent and summed in bfloat16 or wider, within the bound.
No kernel may reach another device: no remote copies, remote signals or barrier semaphores. Data moves between devices by JAX's collectives and lax.ppermute only.
A program may use at most 128 MiB of HBM per device.

v0:
```python
import math
import jax
import jax.numpy as jnp
from jax import lax
from jax.sharding import PartitionSpec as P

HEADS = 16
HD = 64
KV_HEADS = 4
WINDOW = 128
eps = 1e-06


def shifted(block, axis, distance):
    devices = range(lax.axis_size(axis))
    route = [(i - distance, i) for i in devices if i - distance in devices]
    return lax.ppermute(block, axis, route)


def scale_rows(matrix, gain):
    mean_square = jnp.mean(matrix * matrix, axis=-1, keepdims=True)
    return matrix * lax.rsqrt(mean_square + eps) * gain


def per_device(
    queries,
    keys,
    values,
    slopes,
    sinks,
    out_weight,
    mix_gain,
    moe_input,
    in_gain,
    out_gain,
    group_router,
    expert_router,
    routes,
    gate_weight,
    up_weight,
    down_weight,
):
    rows_group = queries.shape[0]
    local_heads = slopes.shape[0]
    per_kv = HEADS // KV_HEADS
    kv_index = lax.axis_index("tp") * local_heads // per_kv
    own_keys = lax.dynamic_slice_in_dim(keys, kv_index * HD, HD, 1)
    own_values = lax.dynamic_slice_in_dim(values, kv_index * HD, HD, 1)
    rim_keys, rim_values = shifted(
        (own_keys[rows_group - WINDOW :], own_values[rows_group - WINDOW :]), "ep", 1
    )
    blocks = rows_group // WINDOW
    key_blocks = own_keys.reshape(blocks, WINDOW, HD)
    value_blocks = own_values.reshape(blocks, WINDOW, HD)
    key_span = jnp.concatenate(
        [jnp.concatenate([rim_keys[None], key_blocks[:-1]], axis=0), key_blocks], axis=1
    )
    value_span = jnp.concatenate(
        [jnp.concatenate([rim_values[None], value_blocks[:-1]], axis=0), value_blocks], axis=1
    )
    query_blocks = queries.reshape(blocks, WINDOW, local_heads, HD)
    scores = jnp.einsum(
        "nqhd,nsd->nhqs", query_blocks, key_span, preferred_element_type=jnp.float32
    ) * (1.0 / math.sqrt(HD))
    query_index = jnp.arange(WINDOW, dtype=jnp.int32)[:, None]
    key_index = jnp.arange(2 * WINDOW, dtype=jnp.int32)[None, :]
    distance = query_index + WINDOW - key_index
    key_position = (
        lax.axis_index("ep") * rows_group
        + jnp.arange(blocks, dtype=jnp.int32)[:, None, None] * WINDOW
        + key_index[None]
        - WINDOW
    )
    valid = ((distance >= 0) & (distance < WINDOW))[None] & (key_position >= 0)
    scores = scores - slopes[None, :, None, None] * distance.astype(jnp.float32)[None, None]
    scores = jnp.where(valid[:, None], scores, -jnp.inf)
    sink = sinks[None, :, None, None]
    top = jnp.maximum(jnp.max(scores, axis=-1, keepdims=True), sink)
    weights = jnp.exp(scores - top)
    denom = jnp.sum(weights, axis=-1, keepdims=True) + jnp.exp(sink - top)
    probs = (weights / denom).astype(jnp.bfloat16)
    attention = jnp.einsum("nhqs,nsd->nqhd", probs, value_span, preferred_element_type=jnp.float32)
    attention = attention.astype(jnp.bfloat16).reshape(rows_group, local_heads * HD)
    own_rows = moe_input.shape[0]
    projected = lax.psum_scatter(
        jnp.dot(attention, out_weight, preferred_element_type=jnp.float32).astype(jnp.bfloat16),
        "tp",
        scatter_dimension=0,
        tiled=True,
    ).astype(jnp.float32)
    mixer_output = scale_rows(projected, mix_gain).astype(jnp.bfloat16)
    normed = scale_rows(moe_input.astype(jnp.float32), in_gain).astype(jnp.bfloat16)
    group_logits = jnp.dot(normed, group_router, preferred_element_type=jnp.float32)
    expert_logits = jnp.dot(normed, expert_router, preferred_element_type=jnp.float32)
    experts = expert_router.shape[1]
    groups = group_router.shape[1]
    per_group = experts // groups
    visits = routes.shape[1]
    expert_match = routes[:, :, None] == jnp.arange(experts, dtype=jnp.int32)[None, None, :]
    picked_logits = jnp.sum(jnp.where(expert_match, expert_logits[:, None, :], 0.0), axis=-1)
    group_prob = jax.nn.softmax(group_logits, axis=-1)
    group_match = (routes // per_group)[:, :, None] == jnp.arange(groups, dtype=jnp.int32)[
        None, None, :
    ]
    picked_group = jnp.sum(jnp.where(group_match, group_prob[:, None, :], 0.0), axis=-1)
    route_weight = picked_group * jax.nn.softmax(picked_logits, axis=-1)
    capacity = max(2, 3 * own_rows * visits // (2 * experts))
    match_int = expert_match.astype(jnp.int32).reshape(own_rows * visits, experts)
    before = jnp.cumsum(match_int, axis=0) - match_int
    slot = jnp.sum(before * match_int, axis=-1)
    position = (routes.reshape(-1) * capacity + slot).reshape(own_rows, visits)
    slot_ids = jnp.arange(experts * capacity, dtype=jnp.int32)
    placement = jnp.any(position[None, :, :] == slot_ids[:, None, None], axis=-1).astype(
        jnp.bfloat16
    )
    outgoing = jnp.dot(placement, normed, preferred_element_type=jnp.float32).astype(jnp.bfloat16)
    local_experts = gate_weight.shape[0]
    outgoing = outgoing.reshape(lax.axis_size("ep"), local_experts, capacity, normed.shape[1])
    arrived = lax.all_to_all(outgoing, "ep", split_axis=0, concat_axis=0, tiled=True)
    gate_piece = lax.all_gather(gate_weight, "tp", axis=2, tiled=True)
    up_piece = lax.all_gather(up_weight, "tp", axis=2, tiled=True)
    down_piece = lax.all_gather(down_weight, "tp", axis=2, tiled=True)
    gate = jnp.einsum("sxcd,xdf->sxcf", arrived, gate_piece, preferred_element_type=jnp.float32)
    up = jnp.einsum("sxcd,xdf->sxcf", arrived, up_piece, preferred_element_type=jnp.float32)
    hidden = (jax.nn.silu(gate) * up).astype(jnp.bfloat16)
    results = jnp.einsum("sxcf,xdf->sxcd", hidden, down_piece, preferred_element_type=jnp.float32)
    returned = lax.all_to_all(
        results.astype(jnp.bfloat16), "ep", split_axis=0, concat_axis=0, tiled=True
    )
    flat_back = returned.reshape(experts * capacity, returned.shape[3])
    picked_rows = jnp.take(flat_back, position.reshape(-1), axis=0).reshape(
        own_rows, visits, flat_back.shape[1]
    )
    moe = jnp.sum(route_weight[:, :, None] * picked_rows.astype(jnp.float32), axis=1)
    moe_output = scale_rows(moe, out_gain).astype(jnp.bfloat16)
    return (mixer_output, moe_output)


def solution(mesh):
    return jax.shard_map(
        per_device,
        mesh=mesh,
        in_specs=(
            P("ep", "tp"),
            P("ep", None),
            P("ep", None),
            P("tp"),
            P("tp"),
            P("tp", None),
            P(),
            P(("ep", "tp"), None),
            P(),
            P(),
            P(),
            P(),
            P(("ep", "tp"), None),
            P("ep", None, "tp"),
            P("ep", None, "tp"),
            P("ep", None, "tp"),
        ),
        out_specs=(P(("ep", "tp"), None), P(("ep", "tp"), None)),
        check_vma=False,
    )
```

profile of v0, /device:TPU:0, one launch (start us, length us, event | category | flops | bytes accessed | tf_op | source)
XLA Modules:
  0.0 222.8 jit_solution(3067624268574023449)
XLA Ops:
  7.2 0.7 all-gather.6.cloned.1.call-update
  8.0 0.7 all-gather.4.cloned.1.call-update
  8.7 0.7 all-gather.8.cloned.1.call-update
  9.5 1.2 constant_dynamic-slice_fusion
  10.9 4.9 %collective-permute-start.1 = (bf16[128,64]{0,1:T(8,128)(2,1)S(1)}, bf16[128,64]{0,1:T(8,128)(2,1)S(1)}, u32[]{:S(2)}, u32[]{:S(2)}) collective-permute-start(bf16[128,64]{0,1:T(8,128)(2,1)S(1)} %slice.36), channel_id=1, source_target_pairs={{0,8},{8,16},{16,24},{1,9},{9,17},{17,25},{2,10},{10,18},{18,26},{... | collective-permute-start | bytes 49160 | tf_op jit(solution)/shard_map/ppermute | solution.py:17
  15.9 3.4 %collective-permute-start = (bf16[128,64]{0,1:T(8,128)(2,1)S(1)}, bf16[128,64]{0,1:T(8,128)(2,1)S(1)}, u32[]{:S(2)}, u32[]{:S(2)}) collective-permute-start(bf16[128,64]{0,1:T(8,128)(2,1)S(1)} %slice.34), channel_id=1, source_target_pairs={{0,8},{8,16},{16,24},{1,9},{9,17},{17,25},{2,10},{10,18},{18,26},{... | collective-permute-start | bytes 49160 | tf_op jit(solution)/shard_map/ppermute | solution.py:17
  19.6 0.3 broadcast_and_fusion
  20.1 0.2 reshape.313
  20.3 0.6 fusion.73
  21.1 0.3 fusion.13
  21.5 0.5 fusion.20
  22.2 3.2 %convolution_convert_fusion = bf16[1024,2048]{1,0:T(8,128)(2,1)} fusion(bf16[128,2048]{1,0:T(8,128)(2,1)S(1)} %copy-done, bf16[16,8,8,128]{3,2,1,0:T(8,128)(2,1)S(1)} %bitcast.155), kind=kOutput, calls=%fused_computation.7 | convolution fusion | flops 538968064 | bytes 4980736 | tf_op jit(solution)/shard_map/dot_general | solution.py:86
  25.4 0.6 copy-done.3
  26.5 1.2 reduce-window.6
  28.6 1.8 convolution_convert_fusion.1
  30.4 3.9 %all-to-all-start = ((bf16[4,1,96,2048]{3,2,1,0:T(8,128)(2,1)}), bf16[4,1,96,2048]{3,2,1,0:T(8,128)(2,1)S(1)}, u32[]{:S(2)}, u32[]{:S(2)}) async-start(bf16[4,1,96,2048]{3,2,1,0:T(8,128)(2,1)} %bitcast.11), calls=%async_computation.1 | async-start | bytes 3145728 | tf_op jit(solution)/shard_map/all_to_all | solution.py:119
  34.3 0.3 fusion.74
  34.7 0.3 fusion.68
  35.5 17.6 %all-to-all-done = bf16[4,1,96,2048]{3,2,1,0:T(8,128)(2,1)S(1)} async-done(((bf16[4,1,96,2048]{3,2,1,0:T(8,128)(2,1)}), bf16[4,1,96,2048]{3,2,1,0:T(8,128)(2,1)S(1)}, u32[]{:S(2)}, u32[]{:S(2)}) %all-to-all-start) | async-done | bytes 1572896 | tf_op jit(solution)/shard_map/all_to_all | solution.py:119
  53.1 7.1 %all-gather.6.cloned.1.call-done = bf16[1,2048,1024]{2,1,0:T(8,128)(2,1)} async-done(((bf16[1,2048,128]{2,1,0:T(8,128)(2,1)}), bf16[1,2048,1024]{2,1,0:T(8,128)(2,1)}) %all-gather.6.cloned.1.call-update) | async-done | bytes 4194320 | tf_op jit(solution)/shard_map/all_gather | solution.py:121
  60.2 5.1 %fusion.2 = f32[4,96,1024]{2,1,0:T(8,128)} fusion(bf16[1,2048,1024]{2,1,0:T(8,128)(2,1)} %all-gather.6.cloned.1.call-done, bf16[4,1,96,2048]{3,2,1,0:T(8,128)(2,1)S(1)} %all-to-all-done), kind=kOutput, calls=%fused_computation.3 | convolution fusion | flops 1610612736 | bytes 7340032 | tf_op jit(solution)/shard_map/sxcd,xdf->sxcf/dot_general | solution.py:124
  65.3 42.5 %all-gather.4.cloned.1.call-done = bf16[1,2048,1024]{2,1,0:T(8,128)(2,1)} async-done(((bf16[1,2048,128]{2,1,0:T(8,128)(2,1)}), bf16[1,2048,1024]{2,1,0:T(8,128)(2,1)}) %all-gather.4.cloned.1.call-update) | async-done | bytes 4194320 | tf_op jit(solution)/shard_map/all_gather | solution.py:120
  107.8 47.6 %all-gather.8.cloned.1.call-done = bf16[1,2048,1024]{2,1,0:T(8,128)(2,1)} async-done(((bf16[1,2048,128]{2,1,0:T(8,128)(2,1)}), bf16[1,2048,1024]{2,1,0:T(8,128)(2,1)}) %all-gather.8.cloned.1.call-update) | async-done | bytes 4194320 | tf_op jit(solution)/shard_map/all_gather | solution.py:122
  155.4 8.6 %fusion.9 = bf16[4,1,96,2048]{3,2,1,0:T(8,128)(2,1)} fusion(bf16[1,2048,1024]{2,1,0:T(8,128)(2,1)} %all-gather.8.cloned.1.call-done, f32[4,96,1024]{2,1,0:T(8,128)} %fusion.2, bf16[1,2048,1024]{2,1,0:T(8,128)(2,1)} %all-gather.4.cloned.1.call-done, bf16[4,1,96,2048]{3,2,1,0:T(8,128)(2,1)S(1)} %all-to-all-done), kind=kOutput, calls=%fused_computation.10 | convolution fusion | flops 3224371200 | bytes 13107200 | tf_op jit(solution)/shard_map/sxcf,xdf->sxcd/dot_general | solution.py:126
  164.1 3.9 %all-to-all-start.1 = ((bf16[4,1,96,2048]{3,2,1,0:T(8,128)(2,1)}), bf16[4,1,96,2048]{3,2,1,0:T(8,128)(2,1)S(1)}, u32[]{:S(2)}, u32[]{:S(2)}) async-start(bf16[4,1,96,2048]{3,2,1,0:T(8,128)(2,1)} %fusion.9), calls=%async_computation.2 | async-start | bytes 3145728 | tf_op jit(solution)/shard_map/all_to_all | solution.py:127
  168.1 37.6 %reduce-scatter.2.cloned.1.call-done = bf16[128,2048]{1,0:T(8,128)(2,1)} async-done(((bf16[1024,2048]{1,0:T(8,128)(2,1)}), bf16[128,2048]{1,0:T(8,128)(2,1)}) %reduce-scatter.2.cloned.1.call-update) | async-done | bytes 524304 | tf_op jit(solution)/shard_map/reduce_scatter | solution.py:85
  205.7 1.2 fusion.30
  207.0 2.0 fusion.32
  209.0 1.4 gather_fusion
  210.4 0.7 gather.7
  211.1 4.1 %multiply_reduce_fusion = f32[128,2048]{1,0:T(8,128)S(1)} fusion(bf16[128,2,2048]{2,1,0:T(2,128)(2,1)S(1)} %gather.7, pred[128,2]{1,0:T(8,128)(4,1)S(1)} %copy.102, f32[128,2]{1,0:T(8,128)S(1)} %copy.96), kind=kLoop, calls=%fused_computation.13 | loop fusion | flops 1835008 | bytes 2098432 | tf_op jit(solution)/shard_map/reduce_sum | solution.py:134
  215.3 1.0 multiply_convert_fusion
  (79 shorter events, 3.2 us)
Async XLA Ops:
  7.2 15.0 %copy-start = (bf16[128,2048]{1,0:T(8,128)(2,1)S(1)}, bf16[128,2048]{1,0:T(8,128)(2,1)}, u32[]{:S(2)}) copy-start(bf16[128,2048]{1,0:T(8,128)(2,1)} %param.21) | copy-start | bytes 1572868
  7.2 53.0 %all-gather.6.cloned.1.call-start = ((), (), s32[]{:S(2)}) async-start(), calls=%async_computation.5 | async-start | bytes 4718592 | tf_op jit(solution)/shard_map/all_gather | solution.py:121
  7.9 12.0 %copy-start.8 = (f32[2]{0:T(128)S(1)}, f32[2]{0:T(128)}, u32[]{:S(2)}) copy-start(f32[2]{0:T(128)} %param.19) | copy-start | bytes 28
  7.9 99.9 %all-gather.4.cloned.1.call-start = ((), (), s32[]{:S(2)}) async-start(), calls=%async_computation.4 | async-start | bytes 4718592 | tf_op jit(solution)/shard_map/all_gather | solution.py:120
  8.7 11.4 %copy-start.2 = (bf16[1024,128]{1,0:T(8,128)(2,1)S(1)}, bf16[1024,128]{1,0:T(8,128)(2,1)}, u32[]{:S(2)}) copy-start(bf16[1024,128]{1,0:T(8,128)(2,1)} %param.16) | copy-start | bytes 786436
  8.7 146.7 %all-gather.8.cloned.1.call-start = ((), (), s32[]{:S(2)}) async-start(), calls=%async_computation.6 | async-start | bytes 4718592 | tf_op jit(solution)/shard_map/all_gather | solution.py:122
  9.4 196.3 %reduce-scatter.2.cloned.1.call-start = ((), (), s32[]{:S(2)}) async-start(), calls=%async_computation.3 | async-start | bytes 4718592 | tf_op jit(solution)/shard_map/reduce_scatter | solution.py:85
  10.9 9.4 %collective-permute-start.1 = (bf16[128,64]{0,1:T(8,128)(2,1)S(1)}, bf16[128,64]{0,1:T(8,128)(2,1)S(1)}, u32[]{:S(2)}, u32[]{:S(2)}) collective-permute-start(bf16[128,64]{0,1:T(8,128)(2,1)S(1)} %slice.36), channel_id=1, source_target_pairs={{0,8},{8,16},{16,24},{1,9},{9,17},{17,25},{2,10},{10,18},{18,26},{... | collective-permute-start | bytes 49160 | tf_op jit(solution)/shard_map/ppermute | solution.py:17
  15.9 5.6 %collective-permute-start = (bf16[128,64]{0,1:T(8,128)(2,1)S(1)}, bf16[128,64]{0,1:T(8,128)(2,1)S(1)}, u32[]{:S(2)}, u32[]{:S(2)}) collective-permute-start(bf16[128,64]{0,1:T(8,128)(2,1)S(1)} %slice.34), channel_id=1, source_target_pairs={{0,8},{8,16},{16,24},{1,9},{9,17},{17,25},{2,10},{10,18},{18,26},{... | collective-permute-start | bytes 49160 | tf_op jit(solution)/shard_map/ppermute | solution.py:17
  20.3 0.7 copy-start.7
  25.4 0.7 copy-start.3
  25.4 3.0 %copy-start.1 = (bf16[128,2048]{1,0:T(8,128)(2,1)S(1)}, bf16[128,2048]{1,0:T(8,128)(2,1)}, u32[]{:S(2)}) copy-start(bf16[128,2048]{1,0:T(8,128)(2,1)} %param.23) | copy-start | bytes 1572868
  25.4 3.2 %copy-start.4 = (f32[2048]{0:T(1024)S(1)}, f32[2048]{0:T(1024)}, u32[]{:S(2)}) copy-start(f32[2048]{0:T(1024)} %param.24) | copy-start | bytes 24580
  30.4 3.9 %copy-start.9 = (bf16[2048,4]{0,1:T(4,128)(2,1)S(1)}, bf16[2048,4]{0,1:T(4,128)(2,1)}, u32[]{:S(2)}) copy-start(bf16[2048,4]{0,1:T(4,128)(2,1)} %param.26) | copy-start | bytes 49156
  30.4 4.3 %copy-start.10 = (bf16[2048,4]{0,1:T(4,128)(2,1)S(1)}, bf16[2048,4]{0,1:T(4,128)(2,1)}, u32[]{:S(2)}) copy-start(bf16[2048,4]{0,1:T(4,128)(2,1)} %param.27) | copy-start | bytes 49156
  30.4 22.6 %all-to-all-start = ((bf16[4,1,96,2048]{3,2,1,0:T(8,128)(2,1)}), bf16[4,1,96,2048]{3,2,1,0:T(8,128)(2,1)S(1)}, u32[]{:S(2)}, u32[]{:S(2)}) async-start(bf16[4,1,96,2048]{3,2,1,0:T(8,128)(2,1)} %bitcast.11), calls=%async_computation.1 | async-start | bytes 3145728 | tf_op jit(solution)/shard_map/all_to_all | solution.py:119
  164.1 42.9 %copy-start.5 = (f32[2048]{0:T(1024)S(1)}, f32[2048]{0:T(1024)}, u32[]{:S(2)}) copy-start(f32[2048]{0:T(1024)} %param.22) | copy-start | bytes 24580
  164.1 44.9 %all-to-all-start.1 = ((bf16[4,1,96,2048]{3,2,1,0:T(8,128)(2,1)}), bf16[4,1,96,2048]{3,2,1,0:T(8,128)(2,1)S(1)}, u32[]{:S(2)}, u32[]{:S(2)}) async-start(bf16[4,1,96,2048]{3,2,1,0:T(8,128)(2,1)} %fusion.9), calls=%async_computation.2 | async-start | bytes 3145728 | tf_op jit(solution)/shard_map/all_to_all | solution.py:127
  211.1 4.3 %copy-start.6 = (f32[2048]{0:T(1024)S(1)}, f32[2048]{0:T(1024)}, u32[]{:S(2)}) copy-start(f32[2048]{0:T(1024)} %param.25) | copy-start | bytes 24580
Sparse Core Ops, SparseCore 0:
  9.6 50.5 all-gather.5
  61.7 45.9 all-gather.3
  109.4 45.9 all-gather.7
  157.6 48.1 reduce-scatter.1
where the time goes:
time: 223 us
  waiting for transfers between devices  155 us (70%)
  matrix products  20.5 us (9%)
  starting transfers between devices  16.2 us (7%)
  between operations  14.2 us (6%)
  other arithmetic  11.3 us (5%)
  local copies, waits for them, and re-layouts  6.18 us (3%)
    all_gather x1, waiting for transfers between devices, per_device(): down_piece = lax.all_gather(down_weight, 'tp', axis=2, tiled=True)  47.6 us
    all_gather x1, waiting for transfers between devices, per_device(): gate_piece = lax.all_gather(gate_weight, 'tp', axis=2, tiled=True)  42.5 us
    reduce_scatter x1, waiting for transfers between devices, per_device(): lax.psum_scatter(jnp.dot(attention, out_weight, preferred_element_type=jn...  37.6 us
    all_to_all x1, waiting for transfers between devices, per_device(): lax.all_to_all(outgoing, 'ep', split_axis=0, concat_axis=0, tiled=True)  17.6 us
    dot_general x1, matrix products, per_device(): jnp.einsum('sxcf,xdf->sxcd', hidden, down_piece, preferred_element_type=j...  8.63 us
    ppermute x2, starting transfers between devices, shifted(): return lax.ppermute(block, axis, route)  8.27 us
    all_gather x1, waiting for transfers between devices, per_device(): up_piece = lax.all_gather(up_weight, 'tp', axis=2, tiled=True)  7.09 us
    dot_general x1, matrix products, per_device(): jnp.einsum('sxcd,xdf->sxcf', arrived, up_piece, preferred_element_type=jn...  5.13 us
  transfers between devices with their start and end apart: 8, of which 5 were waited for; matrix products, arithmetic and copies ran while one was open for 13% of the time, Pallas kernels for 0%

commit v1 on v0

--- a/solution.py
+++ b/solution.py
@@ -1,3 +1,4 @@
+import functools
 import math
 import jax
 import jax.numpy as jnp
@@ -9,6 +10,25 @@
 KV_HEADS = 4
 WINDOW = 128
 eps = 1e-06
+
+
+def settle_the_tails(view, link_axis):
+    r2, r1, lower = (jax.lax.axis_size(link_axis), jax.lax.axis_index(link_axis), view.shape[2])
+    m_next = lax.dynamic_update_slice_in_dim(
+        jnp.zeros([idx * r2 if at == 2 else idx for at, idx in enumerate(view.shape)], view.dtype),
+        view,
+        r1 * lower,
+        axis=2,
+    )
+    h = 1
+    while h < r2:
+        view = jax.lax.ppermute(view, link_axis, [(at, (at + 1) % r2) for at in range(r2)])
+        m_next = lax.dynamic_update_slice_in_dim(m_next, view, (r1 - h) % r2 * lower, axis=2)
+        h += 1
+    return m_next
+
+
+write_limits = functools.partial(settle_the_tails, link_axis="tp")
 
 
 def shifted(block, axis, distance):
@@ -117,7 +137,7 @@
     local_experts = gate_weight.shape[0]
     outgoing = outgoing.reshape(lax.axis_size("ep"), local_experts, capacity, normed.shape[1])
     arrived = lax.all_to_all(outgoing, "ep", split_axis=0, concat_axis=0, tiled=True)
-    gate_piece = lax.all_gather(gate_weight, "tp", axis=2, tiled=True)
+    gate_piece = write_limits(gate_weight)
     up_piece = lax.all_gather(up_weight, "tp", axis=2, tiled=True)
     down_piece = lax.all_gather(down_weight, "tp", axis=2, tiled=True)
     gate = jnp.einsum("sxcd,xdf->sxcf", arrived, gate_piece, preferred_element_type=jnp.float32)

time: 223 us -> 195 us (0.87)
  waiting for transfers between devices: 155 us -> 113 us
  local copies, waits for them, and re-layouts: 6.18 us -> 17.9 us
    ppermute x0 -> x7, waiting for transfers between devices: none -> 88 us  [settle_the_tails(): jax.lax.ppermute(view, link_axis, [(at, (at + 1) % r2) for at in range(r2)])]
    all_gather x1, waiting for transfers between devices: 47.6 us -> 0.01 us  [per_device(): down_piece = lax.all_gather(down_weight, 'tp', axis=2, tiled=True)]
    all_gather x1 -> x0, waiting for transfers between devices: 42.5 us -> none  [per_device(): gate_piece = lax.all_gather(gate_weight, 'tp', axis=2, tiled=True)]
    all_to_all x1, waiting for transfers between devices: 17.6 us -> 0.01 us  [per_device(): lax.all_to_all(outgoing, 'ep', split_axis=0, concat_axis=0, tiled=True)]
    reduce_scatter x1, waiting for transfers between devices: 37.6 us -> 23.7 us  [per_device(): lax.psum_scatter(jnp.dot(attention, out_weight, preferred_element_type=jn...]
    dynamic_update_slice x0 -> x8, local copies, waits for them, and re-layouts: none -> 9.19 us  [the longest x7 8.25 us: settle_the_tails(): lax.dynamic_update_slice_in_dim(m_next, view, (r1 - h) % r2 * lower, axis=2)]
    all_gather x1, waiting for transfers between devices: 7.09 us -> 0.01 us  [per_device(): up_piece = lax.all_gather(up_weight, 'tp', axis=2, tiled=True)]
    another operation x2 -> x3, local copies, waits for them, and re-layouts: 0.1 us -> 2.59 us
  transfers between devices with their start and end apart: 8 -> 14, of which waited for: 5 -> 7; matrix products, arithmetic and copies ran while one was open for 13% -> 22% of each run, Pallas kernels for 0% -> 0%
where the time goes in v1:
time: 195 us
  waiting for transfers between devices  113 us (58%)
  matrix products  20.8 us (11%)
  local copies, waits for them, and re-layouts  17.9 us (9%)
  starting transfers between devices  17.3 us (9%)
  between operations  14.2 us (7%)
  other arithmetic  11.2 us (6%)
    ppermute x7, waiting for transfers between devices, settle_the_tails(): jax.lax.ppermute(view, link_axis, [(at, (at + 1) % r2) for at in range(r2)])  88 us
    reduce_scatter x1, waiting for transfers between devices, per_device(): lax.psum_scatter(jnp.dot(attention, out_weight, preferred_element_type=jn...  23.7 us
    dot_general x1, matrix products, per_device(): jnp.einsum('sxcf,xdf->sxcd', hidden, down_piece, preferred_element_type=j...  8.86 us
    dynamic_update_slice x7, local copies, waits for them, and re-layouts, settle_the_tails(): lax.dynamic_update_slice_in_dim(m_next, view, (r1 - h) % r2 * lower, axis=2)  8.25 us
    ppermute x2, starting transfers between devices, shifted(): return lax.ppermute(block, axis, route)  7.82 us
    dot_general x1, matrix products, per_device(): jnp.einsum('sxcd,xdf->sxcf', arrived, up_piece, preferred_element_type=jn...  5.13 us
    reduce_sum x1, other arithmetic, per_device(): jnp.sum(route_weight[:, :, None] * picked_rows.astype(jnp.float32), axis=1)  4.07 us
    all_to_all x1, starting transfers between devices, per_device(): lax.all_to_all(results.astype(jnp.bfloat16), 'ep', split_axis=0, concat_a...  4 us
  transfers between devices with their start and end apart: 14, of which 7 were waited for; matrix products, arithmetic and copies ran while one was open for 22% of the time, Pallas kernels for 0%

profile of v1, /device:TPU:0, one launch (start us, length us, event | category | flops | bytes accessed | tf_op | source)
XLA Modules:
  0.0 194.6 jit_solution(6662852009122302607)
XLA Ops:
  9.3 1.2 constant_dynamic-slice_fusion
  10.7 4.4 %collective-permute-start.1 = (bf16[128,64]{0,1:T(8,128)(2,1)S(1)}, bf16[128,64]{0,1:T(8,128)(2,1)S(1)}, u32[]{:S(2)}, u32[]{:S(2)}) collective-permute-start(bf16[128,64]{0,1:T(8,128)(2,1)S(1)} %slice.36), channel_id=1, source_target_pairs={{0,8},{8,16},{16,24},{1,9},{9,17},{17,25},{2,10},{10,18},{18,26},{... | collective-permute-start | bytes 49160 | tf_op jit(solution)/shard_map/ppermute | solution.py:37
  15.3 3.4 %collective-permute-start = (bf16[128,64]{0,1:T(8,128)(2,1)S(1)}, bf16[128,64]{0,1:T(8,128)(2,1)S(1)}, u32[]{:S(2)}, u32[]{:S(2)}) collective-permute-start(bf16[128,64]{0,1:T(8,128)(2,1)S(1)} %slice.34), channel_id=1, source_target_pairs={{0,8},{8,16},{16,24},{1,9},{9,17},{17,25},{2,10},{10,18},{18,26},{... | collective-permute-start | bytes 49160 | tf_op jit(solution)/shard_map/ppermute | solution.py:37
  19.8 1.2 reduce-window.6
  23.5 3.2 %convolution_convert_fusion = bf16[1024,2048]{1,0:T(8,128)(2,1)} fusion(bf16[128,2048]{1,0:T(8,128)(2,1)S(1)} %copy-done, bf16[16,8,8,128]{3,2,1,0:T(8,128)(2,1)S(1)} %bitcast.168), kind=kOutput, calls=%fused_computation.7 | convolution fusion | flops 538968064 | bytes 4980736 | tf_op jit(solution)/shard_map/dot_general | solution.py:106
  28.0 1.8 convolution_convert_fusion.1
  29.8 3.7 %all-to-all-start = ((bf16[4,1,96,2048]{3,2,1,0:T(8,128)(2,1)}), bf16[4,1,96,2048]{3,2,1,0:T(8,128)(2,1)S(1)}, u32[]{:S(2)}, u32[]{:S(2)}) async-start(bf16[4,1,96,2048]{3,2,1,0:T(8,128)(2,1)} %bitcast.20), calls=%async_computation.1 | async-start | bytes 3145728 | tf_op jit(solution)/shard_map/all_to_all | solution.py:139
  33.5 1.1 collective-permute-start.3
  35.3 20.0 %collective-permute-done.3 = bf16[1,2048,128]{2,1,0:T(8,128)(2,1)} collective-permute-done((bf16[1,2048,128]{2,1,0:T(8,128)(2,1)S(1)}, bf16[1,2048,128]{2,1,0:T(8,128)(2,1)}, u32[]{:S(2)}, u32[]{:S(2)}) %collective-permute-start.3) | collective-permute-done | bytes 524320 | tf_op jit(solution)/shard_map/ppermute | solution.py:25
  55.4 14.2 %collective-permute-done.4 = bf16[1,2048,128]{2,1,0:T(8,128)(2,1)S(1)} collective-permute-done((bf16[1,2048,128]{2,1,0:T(8,128)(2,1)}, bf16[1,2048,128]{2,1,0:T(8,128)(2,1)S(1)}, u32[]{:S(2)}, u32[]{:S(2)}) %collective-permute-start.4) | collective-permute-done | bytes 524320 | tf_op jit(solution)/shard_map/ppermute | solution.py:25
  70.0 2.5 %broadcast.267 = bf16[2048,1024]{1,0:T(8,128)(2,1)} broadcast(bf16[]{:T(256)} %constant.144.clone.1), dimensions={} | broadcast | bytes 4194306 | tf_op jit(solution)/shard_map/broadcast.120
  72.5 0.9 bitcast_dynamic-update-slice_fusion.7
  73.5 7.9 %collective-permute-done.5 = bf16[1,2048,128]{2,1,0:T(8,128)(2,1)} collective-permute-done((bf16[1,2048,128]{2,1,0:T(8,128)(2,1)S(1)}, bf16[1,2048,128]{2,1,0:T(8,128)(2,1)}, u32[]{:S(2)}, u32[]{:S(2)}) %collective-permute-start.5) | collective-permute-done | bytes 524320 | tf_op jit(solution)/shard_map/ppermute | solution.py:25
  81.3 0.9 bitcast_dynamic-update-slice_fusion.6
  82.2 1.9 bitcast_dynamic-update-slice_fusion.5
  84.1 18.4 %collective-permute-done.6 = bf16[1,2048,128]{2,1,0:T(8,128)(2,1)S(1)} collective-permute-done((bf16[1,2048,128]{2,1,0:T(8,128)(2,1)}, bf16[1,2048,128]{2,1,0:T(8,128)(2,1)S(1)}, u32[]{:S(2)}, u32[]{:S(2)}) %collective-permute-start.6) | collective-permute-done | bytes 524320 | tf_op jit(solution)/shard_map/ppermute | solution.py:25
  102.5 0.9 bitcast_dynamic-update-slice_fusion.4
  103.4 1.9 bitcast_dynamic-update-slice_fusion.3
  105.3 19.0 %collective-permute-done.7 = bf16[1,2048,128]{2,1,0:T(8,128)(2,1)S(1)} collective-permute-done((bf16[1,2048,128]{2,1,0:T(8,128)(2,1)S(1)}, bf16[1,2048,128]{2,1,0:T(8,128)(2,1)S(1)}, u32[]{:S(2)}, u32[]{:S(2)}) %collective-permute-start.7) | collective-permute-done | bytes 524320 | tf_op jit(solution)/shard_map/ppermute | solution.py:25
  124.3 0.9 bitcast_dynamic-update-slice_fusion.2
  125.1 0.9 bitcast_dynamic-update-slice_fusion.1
  126.0 8.7 %collective-permute-done.8 = bf16[1,2048,128]{2,1,0:T(8,128)(2,1)S(1)} collective-permute-done((bf16[1,2048,128]{2,1,0:T(8,128)(2,1)S(1)}, bf16[1,2048,128]{2,1,0:T(8,128)(2,1)S(1)}, u32[]{:S(2)}, u32[]{:S(2)}) %collective-permute-start.8) | collective-permute-done | bytes 524320 | tf_op jit(solution)/shard_map/ppermute | solution.py:25
  134.7 0.9 bitcast_dynamic-update-slice_fusion
  135.6 5.1 %fusion.2 = f32[4,96,1024]{2,1,0:T(8,128)} fusion(bf16[1,2048,1024]{2,1,0:T(8,128)(2,1)} %all-gather.3.cloned.1.call-done, bf16[4,1,96,2048]{3,2,1,0:T(8,128)(2,1)S(1)} %all-to-all-done), kind=kOutput, calls=%fused_computation.3 | convolution fusion | flops 1610612736 | bytes 7340032 | tf_op jit(solution)/shard_map/sxcd,xdf->sxcf/dot_general | solution.py:144
  140.7 8.9 %fusion.9 = bf16[4,1,96,2048]{3,2,1,0:T(8,128)(2,1)} fusion(bf16[1,2048,1024]{2,1,0:T(8,128)(2,1)} %all-gather.5.cloned.1.call-done, f32[4,96,1024]{2,1,0:T(8,128)} %fusion.2, bf16[4,1,96,2048]{3,2,1,0:T(8,128)(2,1)S(1)} %all-to-all-done, bf16[2048,1024]{1,0:T(8,128)(2,1)} %bitcast_dynamic-update-slice_fusion), kind=kOutput, calls=%fused_computation.10 | convolution fusion | flops 3224371200 | bytes 13107200 | tf_op jit(solution)/shard_map/sxcf,xdf->sxcd/dot_general | solution.py:146
  149.6 4.0 %all-to-all-start.1 = ((bf16[4,1,96,2048]{3,2,1,0:T(8,128)(2,1)}), bf16[4,1,96,2048]{3,2,1,0:T(8,128)(2,1)S(1)}, u32[]{:S(2)}, u32[]{:S(2)}) async-start(bf16[4,1,96,2048]{3,2,1,0:T(8,128)(2,1)} %fusion.9), calls=%async_computation.2 | async-start | bytes 3145728 | tf_op jit(solution)/shard_map/all_to_all | solution.py:147
  153.8 23.7 %reduce-scatter.2.cloned.1.call-done = bf16[128,2048]{1,0:T(8,128)(2,1)} async-done(((bf16[1024,2048]{1,0:T(8,128)(2,1)}), bf16[128,2048]{1,0:T(8,128)(2,1)}) %reduce-scatter.2.cloned.1.call-update) | async-done | bytes 524304 | tf_op jit(solution)/shard_map/reduce_scatter | solution.py:105
  177.5 1.2 fusion.21
  178.7 2.0 %fusion.23 = bf16[128,2048]{1,0:T(8,128)(2,1)} fusion(bf16[128,2048]{1,0:T(8,128)(2,1)} %reduce-scatter.2.cloned.1.call-done, f32[2048]{0:T(1024)S(1)} %copy-done.6, f32[128]{0:T(128)S(1)} %add_rsqrt_fusion.2), kind=kLoop, calls=%fused_computation.35 | loop fusion | flops 1048576 | bytes 1057280 | tf_op jit(solution)/shard_map/convert_element_type | solution.py:111
  180.7 1.4 gather_fusion
  182.8 4.1 %multiply_reduce_fusion = f32[128,2048]{1,0:T(8,128)S(1)} fusion(bf16[128,2,2048]{2,1,0:T(2,128)(2,1)S(1)} %gather.7, pred[128,2]{1,0:T(8,128)(4,1)S(1)} %copy.102, f32[128,2]{1,0:T(8,128)S(1)} %copy.96), kind=kLoop, calls=%fused_computation.13 | loop fusion | flops 1835008 | bytes 2098432 | tf_op jit(solution)/shard_map/reduce_sum | solution.py:154
  187.1 1.0 multiply_convert_fusion
  (101 shorter events, 9.2 us)
Async XLA Ops:
  7.2 16.3 %copy-start = (bf16[128,2048]{1,0:T(8,128)(2,1)S(1)}, bf16[128,2048]{1,0:T(8,128)(2,1)}, u32[]{:S(2)}) copy-start(bf16[128,2048]{1,0:T(8,128)(2,1)} %param.21) | copy-start | bytes 1572868
  7.2 11.5 %copy-start.4 = (s32[128,2]{0,1:T(2,128)S(1)}, s32[128,2]{0,1:T(2,128)}, u32[]{:S(2)}) copy-start(s32[128,2]{0,1:T(2,128)} %param.28) | copy-start | bytes 3076
  7.2 128.4 %all-gather.3.cloned.1.call-start = ((), (), s32[]{:S(2)}) async-start(), calls=%async_computation.4 | async-start | bytes 4718592 | tf_op jit(solution)/shard_map/all_gather | solution.py:141
  7.9 11.6 %copy-start.9 = (f32[2]{0:T(128)S(1)}, f32[2]{0:T(128)}, u32[]{:S(2)}) copy-start(f32[2]{0:T(128)} %param.19) | copy-start | bytes 28
  7.9 132.8 %all-gather.5.cloned.1.call-start = ((), (), s32[]{:S(2)}) async-start(), calls=%async_computation.5 | async-start | bytes 4718592 | tf_op jit(solution)/shard_map/all_gather | solution.py:142
  8.7 12.7 %copy-start.3 = (bf16[1024,128]{1,0:T(8,128)(2,1)S(1)}, bf16[1024,128]{1,0:T(8,128)(2,1)}, u32[]{:S(2)}) copy-start(bf16[1024,128]{1,0:T(8,128)(2,1)} %param.16) | copy-start | bytes 786436
  8.7 168.8 %reduce-scatter.2.cloned.1.call-start = ((), (), s32[]{:S(2)}) async-start(), calls=%async_computation.3 | async-start | bytes 4718592 | tf_op jit(solution)/shard_map/reduce_scatter | solution.py:105
  8.7 24.8 %collective-permute-start.2 = (bf16[1,2048,128]{2,1,0:T(8,128)(2,1)}, bf16[1,2048,128]{2,1,0:T(8,128)(2,1)S(1)}, u32[]{:S(2)}, u32[]{:S(2)}) collective-permute-start(bf16[1,2048,128]{2,1,0:T(8,128)(2,1)} %param.29), channel_id=1, source_target_pairs={{0,1},{1,2},{2,3},{3,4},{4,5},{5,6},{6,7},{7,0},{8,9},{9,10},{10,1... | collective-permute-start | bytes 1572872 | tf_op jit(solution)/shard_map/ppermute | solution.py:25
  10.7 10.9 %collective-permute-start.1 = (bf16[128,64]{0,1:T(8,128)(2,1)S(1)}, bf16[128,64]{0,1:T(8,128)(2,1)S(1)}, u32[]{:S(2)}, u32[]{:S(2)}) collective-permute-start(bf16[128,64]{0,1:T(8,128)(2,1)S(1)} %slice.36), channel_id=1, source_target_pairs={{0,8},{8,16},{16,24},{1,9},{9,17},{17,25},{2,10},{10,18},{18,26},{... | collective-permute-start | bytes 49160 | tf_op jit(solution)/shard_map/ppermute | solution.py:37
  15.3 7.5 %collective-permute-start = (bf16[128,64]{0,1:T(8,128)(2,1)S(1)}, bf16[128,64]{0,1:T(8,128)(2,1)S(1)}, u32[]{:S(2)}, u32[]{:S(2)}) collective-permute-start(bf16[128,64]{0,1:T(8,128)(2,1)S(1)} %slice.34), channel_id=1, source_target_pairs={{0,8},{8,16},{16,24},{1,9},{9,17},{17,25},{2,10},{10,18},{18,26},{... | collective-permute-start | bytes 49160 | tf_op jit(solution)/shard_map/ppermute | solution.py:37
  21.6 0.7 copy-start.8
  26.7 1.0 copy-start.1
  26.7 1.3 copy-start.5
  29.8 4.9 %copy-start.10 = (bf16[2048,4]{0,1:T(4,128)(2,1)S(1)}, bf16[2048,4]{0,1:T(4,128)(2,1)}, u32[]{:S(2)}) copy-start(bf16[2048,4]{0,1:T(4,128)(2,1)} %param.26) | copy-start | bytes 49156
  29.8 5.2 %copy-start.11 = (bf16[2048,4]{0,1:T(4,128)(2,1)S(1)}, bf16[2048,4]{0,1:T(4,128)(2,1)}, u32[]{:S(2)}) copy-start(bf16[2048,4]{0,1:T(4,128)(2,1)} %param.27) | copy-start | bytes 49156
  29.8 105.8 %all-to-all-start = ((bf16[4,1,96,2048]{3,2,1,0:T(8,128)(2,1)}), bf16[4,1,96,2048]{3,2,1,0:T(8,128)(2,1)S(1)}, u32[]{:S(2)}, u32[]{:S(2)}) async-start(bf16[4,1,96,2048]{3,2,1,0:T(8,128)(2,1)} %bitcast.20), calls=%async_computation.1 | async-start | bytes 3145728 | tf_op jit(solution)/shard_map/all_to_all | solution.py:139
  33.5 21.8 %collective-permute-start.3 = (bf16[1,2048,128]{2,1,0:T(8,128)(2,1)S(1)}, bf16[1,2048,128]{2,1,0:T(8,128)(2,1)}, u32[]{:S(2)}, u32[]{:S(2)}) collective-permute-start(bf16[1,2048,128]{2,1,0:T(8,128)(2,1)S(1)} %collective-permute-done.2), channel_id=1, source_target_pairs={{0,1},{1,2},{2,3},{3,4},{4,5},{5,6},{6,7},{7,0},{8,9},{9,10},{10,1... | collective-permute-start | bytes 1572872 | tf_op jit(solution)/shard_map/ppermute | solution.py:25
  55.3 14.3 %collective-permute-start.4 = (bf16[1,2048,128]{2,1,0:T(8,128)(2,1)}, bf16[1,2048,128]{2,1,0:T(8,128)(2,1)S(1)}, u32[]{:S(2)}, u32[]{:S(2)}) collective-permute-start(bf16[1,2048,128]{2,1,0:T(8,128)(2,1)} %collective-permute-done.3), channel_id=1, source_target_pairs={{0,1},{1,2},{2,3},{3,4},{4,5},{5,6},{6,7},{7,0},{8,9},{9,10},{10,1... | collective-permute-start | bytes 1572872 | tf_op jit(solution)/shard_map/ppermute | solution.py:25
  69.6 11.7 %collective-permute-start.5 = (bf16[1,2048,128]{2,1,0:T(8,128)(2,1)S(1)}, bf16[1,2048,128]{2,1,0:T(8,128)(2,1)}, u32[]{:S(2)}, u32[]{:S(2)}) collective-permute-start(bf16[1,2048,128]{2,1,0:T(8,128)(2,1)S(1)} %collective-permute-done.4), channel_id=1, source_target_pairs={{0,1},{1,2},{2,3},{3,4},{4,5},{5,6},{6,7},{7,0},{8,9},{9,10},{10,1... | collective-permute-start | bytes 1572872 | tf_op jit(solution)/shard_map/ppermute | solution.py:25
  70.0 2.5 %copy-start.2 = (bf16[1,2048,128]{2,1,0:T(8,128)(2,1)S(1)}, bf16[1,2048,128]{2,1,0:T(8,128)(2,1)}, u32[]{:S(2)}) copy-start(bf16[1,2048,128]{2,1,0:T(8,128)(2,1)} %param.29) | copy-start | bytes 1572868
  81.3 21.2 %collective-permute-start.6 = (bf16[1,2048,128]{2,1,0:T(8,128)(2,1)}, bf16[1,2048,128]{2,1,0:T(8,128)(2,1)S(1)}, u32[]{:S(2)}, u32[]{:S(2)}) collective-permute-start(bf16[1,2048,128]{2,1,0:T(8,128)(2,1)} %collective-permute-done.5), channel_id=1, source_target_pairs={{0,1},{1,2},{2,3},{3,4},{4,5},{5,6},{6,7},{7,0},{8,9},{9,10},{10,1... | collective-permute-start | bytes 1572872 | tf_op jit(solution)/shard_map/ppermute | solution.py:25
  102.5 21.7 %collective-permute-start.7 = (bf16[1,2048,128]{2,1,0:T(8,128)(2,1)S(1)}, bf16[1,2048,128]{2,1,0:T(8,128)(2,1)S(1)}, u32[]{:S(2)}, u32[]{:S(2)}) collective-permute-start(bf16[1,2048,128]{2,1,0:T(8,128)(2,1)S(1)} %collective-permute-done.6), channel_id=1, source_target_pairs={{0,1},{1,2},{2,3},{3,4},{4,5},{5,6},{6,7},{7,0},{8,9},{9,10},{10,1... | collective-permute-start | bytes 1572872 | tf_op jit(solution)/shard_map/ppermute | solution.py:25
  124.3 10.4 %collective-permute-start.8 = (bf16[1,2048,128]{2,1,0:T(8,128)(2,1)S(1)}, bf16[1,2048,128]{2,1,0:T(8,128)(2,1)S(1)}, u32[]{:S(2)}, u32[]{:S(2)}) collective-permute-start(bf16[1,2048,128]{2,1,0:T(8,128)(2,1)S(1)} %collective-permute-done.7), channel_id=1, source_target_pairs={{0,1},{1,2},{2,3},{3,4},{4,5},{5,6},{6,7},{7,0},{8,9},{9,10},{10,1... | collective-permute-start | bytes 1572872 | tf_op jit(solution)/shard_map/ppermute | solution.py:25
  149.6 29.1 %copy-start.6 = (f32[2048]{0:T(1024)S(1)}, f32[2048]{0:T(1024)}, u32[]{:S(2)}) copy-start(f32[2048]{0:T(1024)} %param.22) | copy-start | bytes 24580
  149.6 31.1 %all-to-all-start.1 = ((bf16[4,1,96,2048]{3,2,1,0:T(8,128)(2,1)}), bf16[4,1,96,2048]{3,2,1,0:T(8,128)(2,1)S(1)}, u32[]{:S(2)}, u32[]{:S(2)}) async-start(bf16[4,1,96,2048]{3,2,1,0:T(8,128)(2,1)} %fusion.9), calls=%async_computation.2 | async-start | bytes 3145728 | tf_op jit(solution)/shard_map/all_to_all | solution.py:147
  182.8 4.3 %copy-start.7 = (f32[2048]{0:T(1024)S(1)}, f32[2048]{0:T(1024)}, u32[]{:S(2)}) copy-start(f32[2048]{0:T(1024)} %param.25) | copy-start | bytes 24580
Sparse Core Ops, SparseCore 0:
  9.6 59.0 all-gather.2
  70.3 56.5 all-gather.4
  129.1 48.2 reduce-scatter.1
